TPU v7x, 32 devices: a whole 2x2x4 slice. The times are simulated.
32 devices in a mesh: ep: 32 (over z, y, x, core).
Axes of the slice: x: 2, y: 2, z: 4, core: 2. Of those that a mesh axis runs over, the one named last changes fastest.
Arguments:
- tokens: bfloat16 [128, 4, 1024], P('ep'), may hold values from -6 to 6
- lengths: int32 [128], P('ep'), may hold values from 1 to 4, 192 in all
- routes: int32 [128, 4, 8], P('ep'), may hold values from 0 to 63, all different within a row; in each aligned block of 16 rows (0 to 15, 16 to 31, ...) at most 4 rows name the same one
- gates: float32 [128, 4, 8], P('ep'), may hold values from 0.05 to 0.6
- norm_gain: float32 [1024], replicated, may hold values from 0.5 to 1.5
- expert_gate: bfloat16 [64, 1024, 256], P('ep'), may hold values from -0.1875 to 0.1875
- expert_up: bfloat16 [64, 1024, 256], P('ep'), may hold values from -0.1875 to 0.1875
- expert_down: bfloat16 [64, 256, 1024], P('ep'), may hold values from -0.375 to 0.375
- shared_gate: bfloat16 [1024, 256], replicated, may hold values from -0.1875 to 0.1875
- shared_up: bfloat16 [1024, 256], replicated, may hold values from -0.1875 to 0.1875
- shared_down: bfloat16 [256, 1024], replicated, may hold values from -0.375 to 0.375
- out_gain: float32 [1024], replicated, may hold values from 0.5 to 1.5
Outputs:
- mixed: bfloat16 [128, 4, 1024], P('ep')
Inputs may be any that keep to these rules, and one draw needn't show every extreme that they name: `routes`: in the 16 rows of one device (all slots, in order), no expert is named by more than 4 rows, and some device reaches 4; the experts of one row differ. `lengths`: each sequence has 1 to 4 live slots, the longest exactly 4.
All inputs are finite; a program needn't handle non-finite values.
Results may differ from a plain program's by a relative error of at most 0.0065.
Values may be sent and summed in bfloat16 or wider, within the bound.
A program may use at most 64 MiB of HBM per device.

v0:
```python
import jax
import jax.numpy as jnp
from jax import lax
from jax.sharding import PartitionSpec as P

MOST = 4


EPS = 1e-06


def norm_rows(values, scales):
    wide = values.astype(jnp.float32)
    return wide * lax.rsqrt(jnp.mean(wide * wide, axis=-1, keepdims=True) + EPS) * scales


def run_experts(stacked, expert_gate, expert_up, expert_down):
    gate_part = jnp.einsum("erd,edf->erf", stacked, expert_gate, preferred_element_type=jnp.float32)
    up_part = jnp.einsum("erd,edf->erf", stacked, expert_up, preferred_element_type=jnp.float32)
    hidden = (jax.nn.silu(gate_part) * up_part).astype(jnp.bfloat16)
    return jnp.einsum(
        "erf,efd->erd", hidden, expert_down, preferred_element_type=jnp.float32
    ).astype(jnp.bfloat16)


def padded_path(normed, expert_ids, live_mask, weights, expert_gate, expert_up, expert_down):
    token_count, top_count = expert_ids.shape
    features = normed.shape[1]
    local_count = expert_gate.shape[0]
    devices = lax.axis_size("ep")
    experts_all = local_count * devices
    flat_ids = expert_ids.reshape(-1)
    live_rows = jnp.repeat(live_mask, top_count)
    matches = (
        (flat_ids[:, None] == lax.broadcasted_iota(jnp.int32, (1, experts_all), 1))
        & live_rows[:, None]
    ).astype(jnp.int32)
    earlier = jnp.cumsum(matches, axis=0) - matches
    position = jnp.sum(earlier * matches, axis=1)
    targets = jnp.where(live_rows, flat_ids * MOST + position, experts_all * MOST)
    copies = jnp.repeat(normed, top_count, axis=0)
    outgoing = (
        jnp.zeros((experts_all * MOST, features), jnp.bfloat16).at[targets].set(copies, mode="drop")
    )
    outgoing = outgoing.reshape(devices, local_count * MOST, features)
    arrived = lax.all_to_all(outgoing, "ep", split_axis=0, concat_axis=0, tiled=True)
    stacked = (
        arrived.reshape(devices, local_count, MOST, features)
        .transpose(1, 0, 2, 3)
        .reshape(local_count, devices * MOST, features)
    )
    results = run_experts(stacked, expert_gate, expert_up, expert_down)
    replies = (
        results.reshape(local_count, devices, MOST, features)
        .transpose(1, 0, 2, 3)
        .reshape(devices, local_count * MOST, features)
    )
    returned = lax.all_to_all(replies, "ep", split_axis=0, concat_axis=0, tiled=True)
    returned_flat = returned.reshape(experts_all * MOST, features)
    fetched = returned_flat[jnp.minimum(targets, experts_all * MOST - 1)].reshape(
        token_count, top_count, features
    )
    return jnp.sum(weights[:, :, None] * fetched.astype(jnp.float32), axis=1)


def per_device(
    tokens,
    lengths,
    routes,
    gates,
    norm_gain,
    expert_gate,
    expert_up,
    expert_down,
    shared_gate,
    shared_up,
    shared_down,
    out_gain,
):
    seq_count, new_count, features = tokens.shape
    flat_rows = tokens.reshape(seq_count * new_count, features)
    normed = norm_rows(flat_rows, norm_gain).astype(jnp.bfloat16)
    live_mask = (
        lax.broadcasted_iota(jnp.int32, (seq_count, new_count), 1) < lengths[:, None]
    ).reshape(-1)
    expert_ids = routes.reshape(seq_count * new_count, routes.shape[-1])
    weights = jnp.where(live_mask[:, None], gates.reshape(expert_ids.shape), 0.0)
    routed = padded_path(
        normed, expert_ids, live_mask, weights, expert_gate, expert_up, expert_down
    )
    shared_hidden = (
        jax.nn.silu(jnp.dot(normed, shared_gate, preferred_element_type=jnp.float32))
        * jnp.dot(normed, shared_up, preferred_element_type=jnp.float32)
    ).astype(jnp.bfloat16)
    shared = jnp.dot(shared_hidden, shared_down, preferred_element_type=jnp.float32)
    summed = routed + shared
    mixed_out = jnp.where(live_mask[:, None], norm_rows(summed, out_gain), 0.0)
    return mixed_out.astype(jnp.bfloat16).reshape(tokens.shape)


def solution(mesh):
    placed = (
        P("ep", None, None),
        P("ep"),
        P("ep", None, None),
        P("ep", None, None),
        P(),
        P("ep", None, None),
        P("ep", None, None),
        P("ep", None, None),
        P(),
        P(),
        P(),
        P(),
    )
    return jax.shard_map(
        per_device, mesh=mesh, in_specs=placed, out_specs=P("ep", None, None), check_vma=False
    )
```

profile of v0, /device:TPU:0, one launch (start us, length us, event | category | flops | bytes accessed | tf_op | source)
XLA Modules:
  0.0 55.4 jit_solution(144092994386762034)
XLA Ops:
  0.0 0.8 %iota_compare_fusion.1 = pred[4,4]{1,0:T(4,128)(4,1)S(1)} fusion(s32[4]{0:T(128)} %param.13), kind=kLoop, calls=%fused_computation.40 | loop fusion | flops 16 | bytes 32 | tf_op jit(solution)/shard_map/lt | solution.py:84
  1.2 0.8 %eq.15 = s32[128]{0:T(128)S(1)} reshape(s32[4,4,8]{2,1,0:T(4,128)} %param.14) | data formatting | bytes 1024 | tf_op jit(solution)/shard_map/eq | solution.py:35
  2.0 0.7 %broadcast_multiply_fusion = s32[4,4,8]{2,1,0:T(4,128)S(1)} fusion(s32[4,4,8]{2,1,0:T(4,128)} %param.14), kind=kLoop, calls=%fused_computation.35 | loop fusion | flops 128 | bytes 1024 | tf_op jit(solution)/shard_map/mul | solution.py:40
  2.9 0.2 reduce_window_sum.11
  3.1 0.2 select_reduce_fusion
  3.5 0.6 %copy-done.7 = f32[1024]{0:T(1024)S(1)} copy-done((f32[1024]{0:T(1024)S(1)}, f32[1024]{0:T(1024)}, u32[]{:S(2)}) %copy-start.7) | copy-done | bytes 4120
  4.1 1.3 %scatter_custom_fusion = bf16[256,1024]{1,0:T(8,128)(2,1)S(1)} fusion(s32[128]{0:T(128)S(1)} %get-tuple-element.6, bf16[]{:T(256)} %constant.10.clone.1, bf16[16,1024]{1,0:T(8,128)(2,1)S(1)} %multiply_convert_fusion), kind=kCustom, calls=%fused_computation.10 | custom fusion | bytes 557058 | tf_op jit(solution)/shard_map/scatter | solution.py:43
  5.4 23.5 %all_to_all.10 = bf16[32,8,1024]{2,1,0:T(8,128)(2,1)S(1)} all-to-all(bf16[32,8,1024]{2,1,0:T(8,128)(2,1)S(1)} %bitcast.38), channel_id=1, replica_groups=mesh['ep'=32] {'ep'}, dimensions={0} | all-to-all | bytes 1048576 | tf_op jit(solution)/shard_map/all_to_all | solution.py:46
  28.9 0.3 copy.20
  29.2 0.4 copy.21
  29.8 0.7 %copy-done.1 = bf16[2,1024,256]{2,1,0:T(8,128)(2,1)S(1)} copy-done((bf16[2,1024,256]{2,1,0:T(8,128)(2,1)S(1)}, bf16[2,1024,256]{2,1,0:T(8,128)(2,1)}, u32[]{:S(2)}) %copy-start.1) | copy-done | bytes 1048600
  30.4 0.3 fusion.26
  30.8 1.8 %convolution_convert_fusion = bf16[2,128,1024]{2,1,0:T(8,128)(2,1)S(1)} fusion(bf16[2,256,1024]{2,1,0:T(8,128)(2,1)S(1)} %copy-done, bf16[2,128,1024]{2,1,0:T(8,128)(2,1)S(1)} %reshape.169, bf16[2,1024,256]{2,1,0:T(8,128)(2,1)} %param.18, f32[2,128,256]{2,1,0:T(8,128)S(1)} %fusion.26), kind=kOutput, calls=%fused_computation.2 | convolution fusion | flops 269090816 | bytes 3407872 | tf_op jit(solution)/shard_map/erf,efd->erd/dot_general | solution.py:21
  32.6 0.2 reshape.170
  32.9 1.1 %copy.23 = bf16[32,8,1024]{2,1,0:T(8,128)(2,1)} copy(bf16[32,8,1024]{2,0,1:T(8,128)(2,1)S(1)} %bitcast.40) | data formatting | bytes 1048576 | tf_op jit(solution)/shard_map/reshape | solution.py:56
  34.0 2.7 %all-to-all-start.1 = ((bf16[32,8,1024]{2,1,0:T(8,128)(2,1)}), bf16[32,8,1024]{2,1,0:T(8,128)(2,1)S(1)}, u32[]{:S(2)}, u32[]{:S(2)}) async-start(bf16[32,8,1024]{2,1,0:T(8,128)(2,1)} %copy.23), calls=%async_computation.1 | async-start | bytes 1048576 | tf_op jit(solution)/shard_map/all_to_all | solution.py:58
  36.8 0.7 %copy-done.6 = f32[4,4,8]{2,1,0:T(4,128)S(1)} copy-done((f32[4,4,8]{2,1,0:T(4,128)S(1)}, f32[4,4,8]{2,1,0:T(4,128)}, u32[]{:S(2)}) %copy-start.6) | copy-done | bytes 536
  37.5 0.2 fusion.27
  37.7 14.5 %all-to-all-done.1 = bf16[32,8,1024]{2,1,0:T(8,128)(2,1)S(1)} async-done(((bf16[32,8,1024]{2,1,0:T(8,128)(2,1)}), bf16[32,8,1024]{2,1,0:T(8,128)(2,1)S(1)}, u32[]{:S(2)}, u32[]{:S(2)}) %all-to-all-start.1) | async-done | bytes 524320 | tf_op jit(solution)/shard_map/all_to_all | solution.py:58
  52.2 0.9 %gather_fusion = bf16[128,1024]{1,0:T(8,128)(2,1)S(1)} fusion(bf16[256,1024]{1,0:T(8,128)(2,1)S(1)} %bitcast.37, s32[1024]{0:T(1024)S(1)} %pad_clamp_fusion), kind=kCustom, calls=%fused_computation | custom fusion | bytes 524800 | tf_op jit(solution)/shard_map/gather | solution.py:60
  53.0 0.2 fusion.2
  53.4 0.6 %multiply_reduce_fusion = (f32[16]{0:T(128)S(1)}, f32[16,1024]{1,0:T(8,128)S(1)}) fusion(f32[16,1024]{1,0:T(8,128)S(1)} %fusion.2, bf16[256,1024]{1,0:T(8,128)(2,1)S(1)} %copy-done.3, bf16[16,1024]{1,0:T(8,128)(2,1)S(1)} %multiply_convert_fusion, bf16[1024,256]{1,0:T(8,128)(2,1)S(1)} %copy-done.4, f32[16,256]{1,0:T(8,128)S(1)} %fusion.27), kind=kOutput, calls=%fused_computation.21 | convolution fusion | flops 16850928 | bytes 1228864 | tf_op jit(solution)/shard_map/dot_general | solution.py:95
  54.0 0.7 %copy-done.8 = f32[1024]{0:T(1024)S(1)} copy-done((f32[1024]{0:T(1024)S(1)}, f32[1024]{0:T(1024)}, u32[]{:S(2)}) %copy-start.8) | copy-done | bytes 4120
  54.7 0.6 %reshape.173 = bf16[4,4,1024]{2,1,0:T(4,128)(2,1)} reshape(bf16[16,1024]{1,0:T(8,128)(2,1)S(1)} %select_convert_fusion) | data formatting | bytes 65536 | tf_op jit(solution)/shard_map/reshape | solution.py:98
  (32 shorter events, 1.4 us)
Async XLA Ops:
  0.0 30.8 %copy-start = (bf16[2,256,1024]{2,1,0:T(8,128)(2,1)S(1)}, bf16[2,256,1024]{2,1,0:T(8,128)(2,1)}, u32[]{:S(2)}) copy-start(bf16[2,256,1024]{2,1,0:T(8,128)(2,1)} %param.19) | copy-start | bytes 3145732
  0.0 2.7 %copy-start.5 = (bf16[4,4,1024]{2,1,0:T(4,128)(2,1)S(1)}, bf16[4,4,1024]{2,1,0:T(4,128)(2,1)}, u32[]{:S(2)}) copy-start(bf16[4,4,1024]{2,1,0:T(4,128)(2,1)} %param.12) | copy-start | bytes 98308
  3.4 0.7 %copy-start.7 = (f32[1024]{0:T(1024)S(1)}, f32[1024]{0:T(1024)}, u32[]{:S(2)}) copy-start(f32[1024]{0:T(1024)} %param.16) | copy-start | bytes 12292
  29.2 1.2 %copy-start.1 = (bf16[2,1024,256]{2,1,0:T(8,128)(2,1)S(1)}, bf16[2,1024,256]{2,1,0:T(8,128)(2,1)}, u32[]{:S(2)}) copy-start(bf16[2,1024,256]{2,1,0:T(8,128)(2,1)} %param.17) | copy-start | bytes 3145732
  34.0 3.5 %copy-start.2 = (bf16[1024,256]{1,0:T(8,128)(2,1)S(1)}, bf16[1024,256]{1,0:T(8,128)(2,1)}, u32[]{:S(2)}) copy-start(bf16[1024,256]{1,0:T(8,128)(2,1)} %param.20) | copy-start | bytes 1572868
  34.0 18.2 %all-to-all-start.1 = ((bf16[32,8,1024]{2,1,0:T(8,128)(2,1)}), bf16[32,8,1024]{2,1,0:T(8,128)(2,1)S(1)}, u32[]{:S(2)}, u32[]{:S(2)}) async-start(bf16[32,8,1024]{2,1,0:T(8,128)(2,1)} %copy.23), calls=%async_computation.1 | async-start | bytes 1048576 | tf_op jit(solution)/shard_map/all_to_all | solution.py:58
  36.8 0.7 %copy-start.6 = (f32[4,4,8]{2,1,0:T(4,128)S(1)}, f32[4,4,8]{2,1,0:T(4,128)}, u32[]{:S(2)}) copy-start(f32[4,4,8]{2,1,0:T(4,128)} %param.15) | copy-start | bytes 1540
  52.2 1.1 %copy-start.3 = (bf16[256,1024]{1,0:T(8,128)(2,1)S(1)}, bf16[256,1024]{1,0:T(8,128)(2,1)}, u32[]{:S(2)}) copy-start(bf16[256,1024]{1,0:T(8,128)(2,1)} %param.22) | copy-start | bytes 1572868
  52.2 1.2 %copy-start.4 = (bf16[1024,256]{1,0:T(8,128)(2,1)S(1)}, bf16[1024,256]{1,0:T(8,128)(2,1)}, u32[]{:S(2)}) copy-start(bf16[1024,256]{1,0:T(8,128)(2,1)} %param.21) | copy-start | bytes 1572868
  54.0 0.7 %copy-start.8 = (f32[1024]{0:T(1024)S(1)}, f32[1024]{0:T(1024)}, u32[]{:S(2)}) copy-start(f32[1024]{0:T(1024)} %param.23) | copy-start | bytes 12292
where the time goes:
time: 55.9 us; the launch traced here: 55.4 us
  blocking collectives  23.5 us (42%)
  waiting for transfers between devices  14.5 us (26%)
  local copies, waits for them, and re-layouts  9.12 us (16%)
  matrix products  2.85 us (5%)
  starting transfers between devices  2.73 us (5%)
  other arithmetic  2.55 us (5%)
    all_to_all x1, blocking collectives, padded_path(): lax.all_to_all(outgoing, 'ep', split_axis=0, concat_axis=0, tiled=True)  23.5 us
    all_to_all x1, waiting for transfers between devices, padded_path(): lax.all_to_all(replies, 'ep', split_axis=0, concat_axis=0, tiled=True)  14.5 us
    all_to_all x1, starting transfers between devices, padded_path(): lax.all_to_all(replies, 'ep', split_axis=0, concat_axis=0, tiled=True)  2.73 us
    unnamed x18, local copies, waits for them, and re-layouts  2.73 us
    dot_general x1, matrix products, run_experts(): jnp.einsum('erf,efd->erd', hidden, expert_down, preferred_element_type=jn...  1.79 us
    scatter x1, local copies, waits for them, and re-layouts, padded_path(): jnp.zeros((experts_all * MOST, features), jnp.bfloat16).at[targets]  1.3 us
  transfers between devices with their start and end apart: 1, of which 1 were waited for; matrix products, arithmetic and copies ran while one was open for 0% of the time, Pallas kernels for 0%

commit v1 on v0

v1 whole, which is shorter than its diff:
```python
import functools
import jax
import jax.numpy as jnp
from jax import lax
from jax.experimental import pallas as pl
from jax.experimental.pallas import tpu as pltpu
from jax.sharding import PartitionSpec as P

EPS = 1e-06
META = 128
PLANE = 4
CORES = 2
MESH = pl.DeviceIdType.MESH
ANY = pl.ANY


def silu(v):
    return v / (1.0 + jnp.exp(-v))


def layer_kernel(
    line,
    tokens_ref, lengths_ref, routes_ref, gates_ref, norm_ref,
    eg_hbm, eu_hbm, ed_hbm, sg_hbm, su_hbm, sd_hbm, outgain_ref,
    out_ref,
    rows_scr, meta_scr, got, wg, wu, wd, sg, su, sd, acts, part, got_a, got_b, got_c, shared_scr,
    w_sem, w_send, w_recv, g_recv, z_send, x_send, y_send, d_send,
    a_send, a_recv, b_send, b_recv, c_send, c_recv,
):
    me = lax.axis_index("ep")
    core = lax.rem(me, CORES)
    x_bit = lax.rem(me // CORES, 2)
    y_bit = lax.rem(me // (CORES * 2), 2)
    group = CORES * PLANE
    z = me // group
    low = lax.rem(me, group)
    partner = me + 1 - 2 * core
    x_peer = me + CORES * (1 - 2 * x_bit)
    y_peer = me + 2 * CORES * (1 - 2 * y_bit)

    def z_peer(step):
        return lax.rem(z + step + line, line) * group + low

    seqs, new, feats = tokens_ref.shape
    rows = seqs * new
    top = routes_ref.shape[2]
    local = eg_hbm.shape[0]
    half = line // 2

    barrier = pltpu.get_barrier_semaphore()
    peers = [partner, x_peer, y_peer] + [z_peer(r) for r in range(1, line)]
    for peer in peers:
        pl.semaphore_signal(barrier, inc=1, device_id=(peer,), device_id_type=MESH)

    mine = pl.ds(core * local, local)
    loads = []
    for i, (src, dst) in enumerate(((eg_hbm, wg), (eu_hbm, wu), (ed_hbm, wd))):
        loads.append(pltpu.make_async_copy(src, dst.at[mine], w_sem.at[i]))
    for i, (src, dst) in enumerate(((sg_hbm, sg), (su_hbm, su), (sd_hbm, sd))):
        loads.append(pltpu.make_async_copy(src, dst, w_sem.at[3 + i]))
    for load in loads:
        load.start()

    steps = lax.broadcasted_iota(jnp.int32, (new, top), 0)
    meta_scr[...] = jnp.zeros_like(meta_scr)
    for s in range(seqs):
        at = pl.ds(s * new, new)
        rows_scr[at, :] = tokens_ref[s].astype(jnp.float32)
        live = steps < lengths_ref[s]
        gate = jnp.where(live, gates_ref[s], 0.0)
        high = gate.astype(jnp.bfloat16).astype(jnp.float32)
        meta_scr[at, 0:top] = routes_ref[s].astype(jnp.float32)
        meta_scr[at, top:2 * top] = high
        meta_scr[at, 2 * top:3 * top] = gate - high
    wide = rows_scr[...]
    scale = lax.rsqrt(jnp.mean(wide * wide, axis=-1, keepdims=True) + EPS)
    normed = (wide * scale * norm_ref[...]).astype(jnp.bfloat16)
    got[0, 0, :, 0:feats] = normed
    got[0, 0, :, feats:feats + META] = meta_scr[...].astype(jnp.bfloat16)

    pl.semaphore_wait(barrier, len(peers))

    def send(src, dst, ssem, rsem, peer):
        return pltpu.make_async_remote_copy(
            src_ref=src, dst_ref=dst, send_sem=ssem, recv_sem=rsem,
            device_id=(peer,), device_id_type=MESH,
        )

    z_copy = {
        r: send(got.at[0, 0], got.at[0, r], z_send.at[r], g_recv.at[0, r], z_peer(-r))
        for r in range(1, line)
    }
    x_copy = [send(got.at[0, r], got.at[1, r], x_send.at[r], g_recv.at[1, r], x_peer) for r in range(line)]
    y_copy = [send(got.at[0, r], got.at[2, r], y_send.at[r], g_recv.at[2, r], y_peer) for r in range(line)]
    d_copy = [
        send(got.at[1, r], got.at[3, r], d_send.at[r], g_recv.at[3, r], y_peer)
        if r < half
        else send(got.at[2, r], got.at[3, r], d_send.at[r], g_recv.at[3, r], x_peer)
        for r in range(line)
    ]
    order = sorted(range(line), key=lambda r: (min(r, line - r), r))
    for r in order[1:]:
        z_copy[r].start()
    x_copy[0].start()
    y_copy[0].start()
    w_copy = [
        send(src, dst.at[mine], w_send.at[i], w_recv.at[i], partner)
        for i, (src, dst) in enumerate(((eg_hbm, wg), (eu_hbm, wu), (ed_hbm, wd)))
    ]
    for copy in w_copy:
        copy.start()

    for load in loads[3:]:
        load.wait()
    own = got[0, 0, :, 0:feats]
    s_hidden = (
        silu(jnp.dot(own, sg[...], preferred_element_type=jnp.float32))
        * jnp.dot(own, su[...], preferred_element_type=jnp.float32)
    ).astype(jnp.bfloat16)
    shared_scr[...] = jnp.dot(s_hidden, sd[...], preferred_element_type=jnp.float32)

    def relay(r):
        if r < half:
            x_copy[r].wait_recv()
        else:
            y_copy[r].wait_recv()
        d_copy[r].start()

    for i, r in enumerate(order[1:]):
        z_copy[r].wait_recv()
        x_copy[r].start()
        y_copy[r].start()
        relay(order[i])
    relay(order[-1])
    for r in range(line):
        if r < half:
            y_copy[r].wait_recv()
        else:
            x_copy[r].wait_recv()
    for load in loads[:3]:
        load.wait()
    for copy in w_copy:
        copy.wait_recv()

    experts = local * CORES
    hidden_size = wg.shape[2]
    first = (me // CORES) * experts

    def compute(rels):
        lo, count = rels[0], len(rels)
        m = count * line * rows
        stacked = got[lo:lo + count, :, :, 0:feats].reshape(m, feats)
        meta = got[lo:lo + count, :, :, feats:feats + META].reshape(m, META).astype(jnp.float32)
        ids = meta[:, 0:top]
        gate = meta[:, top:2 * top] + meta[:, 2 * top:3 * top]
        for e in range(experts):
            named = (first + e).astype(jnp.float32)
            weight = jnp.sum(jnp.where(ids == named, gate, 0.0), axis=1, keepdims=True)
            gate_part = jnp.dot(stacked, wg[e], preferred_element_type=jnp.float32)
            up_part = jnp.dot(stacked, wu[e], preferred_element_type=jnp.float32)
            acts[0:m, e * hidden_size:(e + 1) * hidden_size] = (
                silu(gate_part) * up_part * weight
            ).astype(jnp.bfloat16)
        tile = 256
        for c in range(0, feats, tile):
            down = wd[:, :, c:c + tile].reshape(experts * hidden_size, tile)
            outs = jnp.dot(acts[0:m, :], down, preferred_element_type=jnp.float32)
            part[lo:lo + count, :, :, c:c + tile] = outs.reshape(count, line, rows, tile).astype(jnp.bfloat16)

    a_copy = [
        send(part.at[3, r], got_a.at[r], a_send.at[r], a_recv.at[r], x_peer if r < half else y_peer)
        for r in range(line)
    ]
    b_copy = [
        [send(part.at[1 + i, r], got_b.at[i, r], b_send.at[i, r], b_recv.at[i, r], peer) for r in range(line)]
        for i, peer in enumerate((x_peer, y_peer))
    ]
    c_copy = {
        r: send(part.at[0, r], got_c.at[r], c_send.at[r], c_recv.at[r], z_peer(r))
        for r in range(1, line)
    }

    compute((0, 1, 2))
    for r in range(line):
        b_copy[0 if r < half else 1][r].start()
    for r in range(line):
        d_copy[r].wait_recv()
    compute((3,))
    for r in order:
        a_copy[r].start()
    for r in order:
        a_copy[r].wait_recv()
        i = 1 if r < half else 0
        part[1 + i, r] = (
            part[1 + i, r].astype(jnp.float32) + got_a[r].astype(jnp.float32)
        ).astype(jnp.bfloat16)
        b_copy[i][r].start()

    def column(r):
        b_copy[0][r].wait_recv()
        b_copy[1][r].wait_recv()
        return (
            part[0, r].astype(jnp.float32)
            + got_b[0, r].astype(jnp.float32)
            + got_b[1, r].astype(jnp.float32)
        )

    for r in order[1:]:
        part[0, r] = column(r).astype(jnp.bfloat16)
        c_copy[r].start()
    summed = column(0) + shared_scr[...]
    for r in order[1:]:
        c_copy[r].wait_recv()
        summed = summed + got_c[r].astype(jnp.float32)
    scale = lax.rsqrt(jnp.mean(summed * summed, axis=-1, keepdims=True) + EPS)
    rows_scr[...] = summed * scale * outgain_ref[...]
    steps = lax.broadcasted_iota(jnp.int32, (new, feats), 0)
    for s in range(seqs):
        live = steps < lengths_ref[s]
        out_ref[s] = jnp.where(live, rows_scr[pl.ds(s * new, new), :], 0.0).astype(out_ref.dtype)

    for copies in (w_copy, x_copy, y_copy, d_copy, a_copy, b_copy[0], b_copy[1],
                   list(z_copy.values()), list(c_copy.values())):
        for copy in copies:
            copy.wait_send()


def per_device(
    tokens, lengths, routes, gates, norm_gain,
    expert_gate, expert_up, expert_down, shared_gate, shared_up, shared_down, out_gain,
):
    devices = lax.axis_size("ep")
    line = devices // (CORES * PLANE)
    seqs, new, feats = tokens.shape
    rows = seqs * new
    local, _, hidden = expert_gate.shape
    experts = local * CORES
    bf, f32 = jnp.bfloat16, jnp.float32
    vm = pl.BlockSpec(memory_space=pltpu.VMEM)
    hbm = pl.BlockSpec(memory_space=ANY)
    dma = pltpu.SemaphoreType.DMA
    return pl.pallas_call(
        functools.partial(layer_kernel, line),
        out_shape=jax.ShapeDtypeStruct(tokens.shape, tokens.dtype),
        in_specs=[vm, pl.BlockSpec(memory_space=pltpu.SMEM), vm, vm, vm] + [hbm] * 6 + [vm],
        out_specs=vm,
        scratch_shapes=[
            pltpu.VMEM((rows, feats), f32),
            pltpu.VMEM((rows, META), f32),
            pltpu.VMEM((PLANE, line, rows, feats + META), bf),
            pltpu.VMEM((experts, feats, hidden), bf),
            pltpu.VMEM((experts, feats, hidden), bf),
            pltpu.VMEM((experts, hidden, feats), bf),
            pltpu.VMEM(shared_gate.shape, bf),
            pltpu.VMEM(shared_up.shape, bf),
            pltpu.VMEM(shared_down.shape, bf),
            pltpu.VMEM(((PLANE - 1) * line * rows, experts * hidden), bf),
            pltpu.VMEM((PLANE, line, rows, feats), bf),
            pltpu.VMEM((line, rows, feats), bf),
            pltpu.VMEM((2, line, rows, feats), bf),
            pltpu.VMEM((line, rows, feats), bf),
            pltpu.VMEM((rows, feats), f32),
            dma((6,)), dma((3,)), dma((3,)),
            dma((PLANE, line)), dma((line,)), dma((line,)), dma((line,)), dma((line,)),
            dma((line,)), dma((line,)), dma((2, line)), dma((2, line)), dma((line,)), dma((line,)),
        ],
        compiler_params=pltpu.CompilerParams(collective_id=0, has_side_effects=True),
    )(
        tokens, lengths, routes, gates, norm_gain.reshape(1, feats),
        expert_gate, expert_up, expert_down, shared_gate, shared_up, shared_down,
        out_gain.reshape(1, feats),
    )


def solution(mesh):
    split = P("ep", None, None)
    placed = (split, P("ep"), split, split, P(), split, split, split, P(), P(), P(), P())
    return jax.shard_map(
        per_device, mesh=mesh, in_specs=placed, out_specs=split, check_vma=False
    )
```

time: 55.9 us -> 34.1 us (0.61)
  Pallas kernels: 0 us -> 32.4 us
  blocking collectives: 23.5 us -> 0 us
  waiting for transfers between devices: 14.5 us -> 0 us
  local copies, waits for them, and re-layouts: 9.12 us -> 1.39 us
  matrix products: 2.85 us -> 0 us
  starting transfers between devices: 2.73 us -> 0 us
  other arithmetic: 2.55 us -> 0 us
    pallas_call x0 -> x1, Pallas kernels: none -> 32.4 us  [per_device(): pl.pallas_call(functools.partial(layer_kernel, line), out_shape=jax.Shape...]
    all_to_all x1 -> x0, blocking collectives: 23.5 us -> none  [padded_path(): lax.all_to_all(outgoing, 'ep', split_axis=0, concat_axis=0, tiled=True)]
    all_to_all x1 -> x0, waiting for transfers between devices: 14.5 us -> none  [padded_path(): lax.all_to_all(replies, 'ep', split_axis=0, concat_axis=0, tiled=True)]
    dot_general x4 -> x0, matrix products: 2.85 us -> none  [the longest x1 1.79 us: run_experts(): jnp.einsum('erf,efd->erd', hidden, expert_down, preferred_element_type=jn...]
    all_to_all x1 -> x0, starting transfers between devices: 2.73 us -> none  [padded_path(): lax.all_to_all(replies, 'ep', split_axis=0, concat_axis=0, tiled=True)]
    reshape x6 -> x0, local copies, waits for them, and re-layouts: 2.29 us -> none  [the longest x1 1.08 us: padded_path(): replies = results.reshape(local_count, devices, MOST, features).transpose...]
    unnamed x18 -> x1, local copies, waits for them, and re-layouts: 2.73 us -> 1.39 us
    scatter x1 -> x0, local copies, waits for them, and re-layouts: 1.3 us -> none  [padded_path(): jnp.zeros((experts_all * MOST, features), jnp.bfloat16).at[targets]]
  transfers between devices with their start and end apart: 1 -> 0, of which waited for: 1 -> 0; matrix products, arithmetic and copies ran while one was open for 0% -> 0% of each run, Pallas kernels for 0% -> 0%
where the time goes in v1:
time: 34.1 us; the launch traced here: 33.8 us
  Pallas kernels  32.4 us (95%)
  local copies, waits for them, and re-layouts  1.39 us (4%)
    pallas_call x1, Pallas kernels, per_device(): pl.pallas_call(functools.partial(layer_kernel, line), out_shape=jax.Shape...  32.4 us
    unnamed x1, local copies, waits for them, and re-layouts  1.39 us

profile of v1, /device:TPU:0, one launch (start us, length us, event | category | flops | bytes accessed | tf_op | source)
XLA Modules:
  0.0 33.8 jit_solution(3754894319741548172)
XLA Ops:
  0.0 32.4 %shard_map.118 = bf16[4,4,1024]{2,1,0:T(4,128)(2,1)} custom-call(bf16[4,4,1024]{2,1,0:T(4,128)(2,1)} %tokens_ref.1, s32[4]{0:T(128)} %lengths_ref.1, s32[4,4,8]{2,1,0:T(4,128)} %routes_ref.1, f32[4,4,8]{2,1,0:T(4,128)} %gates_ref.1, f32[1,1024]{1,0:T(1,128)} %bitcast.2, bf16[2,1024,256]{2,1,0:T(8,128)(2,1)} %eg_hbm.1, bf16[2,1024,256]{2,1,0:T(8,128)(2,1)} %eu_hbm.1, ...), custom_call_target="tpu_custom_call" | custom-call | tf_op jit(solution)/shard_map/pallas_call | solution.py:242
  32.5 1.4 %copy.14 = bf16[4,4,1024]{2,1,0:T(4,128)(2,1)} copy(bf16[4,4,1024]{2,1,0:T(4,128)(2,1)} %shard_map.118) | data formatting | bytes 65536

commit v2 on v1

--- a/solution.py
+++ b/solution.py
@@ -37,6 +37,7 @@
     partner = me + 1 - 2 * core
     x_peer = me + CORES * (1 - 2 * x_bit)
     y_peer = me + 2 * CORES * (1 - 2 * y_bit)
+    xy_peer = x_peer + y_peer - me
 
     def z_peer(step):
         return lax.rem(z + step + line, line) * group + low
@@ -48,7 +49,7 @@
     half = line // 2
 
     barrier = pltpu.get_barrier_semaphore()
-    peers = [partner, x_peer, y_peer] + [z_peer(r) for r in range(1, line)]
+    peers = [partner, x_peer, y_peer, xy_peer] + [z_peer(r) for r in range(1, line)]
     for peer in peers:
         pl.semaphore_signal(barrier, inc=1, device_id=(peer,), device_id_type=MESH)
 
@@ -92,17 +93,13 @@
     }
     x_copy = [send(got.at[0, r], got.at[1, r], x_send.at[r], g_recv.at[1, r], x_peer) for r in range(line)]
     y_copy = [send(got.at[0, r], got.at[2, r], y_send.at[r], g_recv.at[2, r], y_peer) for r in range(line)]
-    d_copy = [
-        send(got.at[1, r], got.at[3, r], d_send.at[r], g_recv.at[3, r], y_peer)
-        if r < half
-        else send(got.at[2, r], got.at[3, r], d_send.at[r], g_recv.at[3, r], x_peer)
-        for r in range(line)
-    ]
+    d_copy = [send(got.at[0, r], got.at[3, r], d_send.at[r], g_recv.at[3, r], xy_peer) for r in range(line)]
     order = sorted(range(line), key=lambda r: (min(r, line - r), r))
     for r in order[1:]:
         z_copy[r].start()
     x_copy[0].start()
     y_copy[0].start()
+    d_copy[0].start()
     w_copy = [
         send(src, dst.at[mine], w_send.at[i], w_recv.at[i], partner)
         for i, (src, dst) in enumerate(((eg_hbm, wg), (eu_hbm, wu), (ed_hbm, wd)))
@@ -110,33 +107,14 @@
     for copy in w_copy:
         copy.start()
 
-    for load in loads[3:]:
-        load.wait()
-    own = got[0, 0, :, 0:feats]
-    s_hidden = (
-        silu(jnp.dot(own, sg[...], preferred_element_type=jnp.float32))
-        * jnp.dot(own, su[...], preferred_element_type=jnp.float32)
-    ).astype(jnp.bfloat16)
-    shared_scr[...] = jnp.dot(s_hidden, sd[...], preferred_element_type=jnp.float32)
-
-    def relay(r):
-        if r < half:
-            x_copy[r].wait_recv()
-        else:
-            y_copy[r].wait_recv()
-        d_copy[r].start()
-
-    for i, r in enumerate(order[1:]):
+    for r in order[1:]:
         z_copy[r].wait_recv()
         x_copy[r].start()
         y_copy[r].start()
-        relay(order[i])
-    relay(order[-1])
-    for r in range(line):
-        if r < half:
-            y_copy[r].wait_recv()
-        else:
-            x_copy[r].wait_recv()
+        d_copy[r].start()
+    for r in order:
+        x_copy[r].wait_recv()
+        y_copy[r].wait_recv()
     for load in loads[:3]:
         load.wait()
     for copy in w_copy:
@@ -167,10 +145,7 @@
             outs = jnp.dot(acts[0:m, :], down, preferred_element_type=jnp.float32)
             part[lo:lo + count, :, :, c:c + tile] = outs.reshape(count, line, rows, tile).astype(jnp.bfloat16)
 
-    a_copy = [
-        send(part.at[3, r], got_a.at[r], a_send.at[r], a_recv.at[r], x_peer if r < half else y_peer)
-        for r in range(line)
-    ]
+    a_copy = [send(part.at[3, r], got_a.at[r], a_send.at[r], a_recv.at[r], xy_peer) for r in range(line)]
     b_copy = [
         [send(part.at[1 + i, r], got_b.at[i, r], b_send.at[i, r], b_recv.at[i, r], peer) for r in range(line)]
         for i, peer in enumerate((x_peer, y_peer))
@@ -182,42 +157,49 @@
 
     compute((0, 1, 2))
     for r in range(line):
-        b_copy[0 if r < half else 1][r].start()
-    for r in range(line):
         d_copy[r].wait_recv()
     compute((3,))
-    for r in order:
+    far = order[::-1]
+    for r in far:
         a_copy[r].start()
-    for r in order:
-        a_copy[r].wait_recv()
-        i = 1 if r < half else 0
-        part[1 + i, r] = (
-            part[1 + i, r].astype(jnp.float32) + got_a[r].astype(jnp.float32)
-        ).astype(jnp.bfloat16)
-        b_copy[i][r].start()
+    for r in far:
+        b_copy[0][r].start()
+        b_copy[1][r].start()
+
+    for load in loads[3:]:
+        load.wait()
+    own = got[0, 0, :, 0:feats]
+    s_hidden = (
+        silu(jnp.dot(own, sg[...], preferred_element_type=jnp.float32))
+        * jnp.dot(own, su[...], preferred_element_type=jnp.float32)
+    ).astype(jnp.bfloat16)
+    shared_scr[...] = jnp.dot(s_hidden, sd[...], preferred_element_type=jnp.float32)
 
     def column(r):
         b_copy[0][r].wait_recv()
         b_copy[1][r].wait_recv()
+        a_copy[r].wait_recv()
         return (
             part[0, r].astype(jnp.float32)
             + got_b[0, r].astype(jnp.float32)
             + got_b[1, r].astype(jnp.float32)
+            + got_a[r].astype(jnp.float32)
         )
 
-    for r in order[1:]:
+    for r in far[:-1]:
         part[0, r] = column(r).astype(jnp.bfloat16)
         c_copy[r].start()
     summed = column(0) + shared_scr[...]
-    for r in order[1:]:
+    for r in far[:-1]:
         c_copy[r].wait_recv()
         summed = summed + got_c[r].astype(jnp.float32)
     scale = lax.rsqrt(jnp.mean(summed * summed, axis=-1, keepdims=True) + EPS)
-    rows_scr[...] = summed * scale * outgain_ref[...]
-    steps = lax.broadcasted_iota(jnp.int32, (new, feats), 0)
+    mixed = summed * scale * outgain_ref[...]
+    steps = lax.broadcasted_iota(jnp.int32, (rows, feats), 0)
     for s in range(seqs):
-        live = steps < lengths_ref[s]
-        out_ref[s] = jnp.where(live, rows_scr[pl.ds(s * new, new), :], 0.0).astype(out_ref.dtype)
+        dead = (steps >= s * new + lengths_ref[s]) & (steps < (s + 1) * new)
+        mixed = jnp.where(dead, 0.0, mixed)
+    out_ref[...] = mixed.astype(out_ref.dtype)
 
     for copies in (w_copy, x_copy, y_copy, d_copy, a_copy, b_copy[0], b_copy[1],
                    list(z_copy.values()), list(c_copy.values())):
@@ -241,7 +223,7 @@
     dma = pltpu.SemaphoreType.DMA
     return pl.pallas_call(
         functools.partial(layer_kernel, line),
-        out_shape=jax.ShapeDtypeStruct(tokens.shape, tokens.dtype),
+        out_shape=jax.ShapeDtypeStruct((rows, feats), tokens.dtype),
         in_specs=[vm, pl.BlockSpec(memory_space=pltpu.SMEM), vm, vm, vm] + [hbm] * 6 + [vm],
         out_specs=vm,
         scratch_shapes=[
@@ -269,7 +251,7 @@
         tokens, lengths, routes, gates, norm_gain.reshape(1, feats),
         expert_gate, expert_up, expert_down, shared_gate, shared_up, shared_down,
         out_gain.reshape(1, feats),
-    )
+    ).reshape(tokens.shape)
 
 
 def solution(mesh):

time: 34.1 us -> 30.6 us (0.90)
  Pallas kernels: 32.4 us -> 29 us
    pallas_call x1, Pallas kernels: 32.4 us -> 29 us  [per_device(): pl.pallas_call(functools.partial(layer_kernel, line), out_shape=jax.Shape...]
    reshape x0 -> x1, local copies, waits for them, and re-layouts: none -> 1.39 us  [per_device(): return pl.pallas_call(functools.partial(layer_kernel, line), out_shape=ja...]
    unnamed x1 -> x0, local copies, waits for them, and re-layouts: 1.39 us -> none
where the time goes in v2:
time: 30.6 us; the launch traced here: 30.4 us
  Pallas kernels  29 us (95%)
  local copies, waits for them, and re-layouts  1.39 us (5%)
    pallas_call x1, Pallas kernels, per_device(): pl.pallas_call(functools.partial(layer_kernel, line), out_shape=jax.Shape...  29 us
    reshape x1, local copies, waits for them, and re-layouts, per_device(): return pl.pallas_call(functools.partial(layer_kernel, line), out_shape=ja...  1.39 us

profile of v2, /device:TPU:0, one launch (start us, length us, event | category | flops | bytes accessed | tf_op | source)
XLA Modules:
  0.0 30.4 jit_solution(4068850507343659381)
XLA Ops:
  0.0 29.0 %shard_map.118 = bf16[16,1024]{1,0:T(8,128)(2,1)} custom-call(bf16[4,4,1024]{2,1,0:T(4,128)(2,1)} %tokens_ref.1, s32[4]{0:T(128)} %lengths_ref.1, s32[4,4,8]{2,1,0:T(4,128)} %routes_ref.1, f32[4,4,8]{2,1,0:T(4,128)} %gates_ref.1, f32[1,1024]{1,0:T(1,128)} %bitcast.2, bf16[2,1024,256]{2,1,0:T(8,128)(2,1)} %eg_hbm.1, bf16[2,1024,256]{2,1,0:T(8,128)(2,1)} %eu_hbm.1, ...), custom_call_target="tpu_custom_call" | custom-call | tf_op jit(solution)/shard_map/pallas_call | solution.py:224
  29.0 1.4 %reshape.11 = bf16[4,4,1024]{2,1,0:T(4,128)(2,1)} reshape(bf16[16,1024]{1,0:T(8,128)(2,1)} %shard_map.118) | data formatting | bytes 65536 | tf_op jit(solution)/shard_map/reshape | solution.py:254
